TPU v7x, 32 devices: a whole 2x2x4 slice. The times are simulated.
32 devices in a mesh: ep: 8 (over z, x), tp: 4 (over y, core).
Axes of the slice: x: 2, y: 2, z: 4, core: 2. Of those that a mesh axis runs over, the one named last changes fastest.
Arguments:
- queries: bfloat16 [4096, 8, 96], P('ep', 'tp'), may hold values from -240 to 240
- kv_latent: bfloat16 [4096, 128], P(('ep', 'tp')), may hold values from -6 to 6
- rope_key: bfloat16 [4096, 32], P(('ep', 'tp')), may hold values from -6 to 6
- kv_gain: float32 [128], replicated, may hold values from 0.1 to 1.9
- kv_up: bfloat16 [128, 8, 128], P(None, 'tp'), may hold values from -0.5 to 0.5
- mix_out: bfloat16 [8, 64, 2048], P('tp'), may hold values from -0.25 to 0.25
- moe_in: bfloat16 [2048, 2048], P('ep', 'tp'), may hold values from -6 to 6
- moe_gain: float32 [2048], replicated, may hold values from 0.1 to 1.9
- routes: int32 [2048, 2], P('ep'), may hold values from 0 to 7, all different within a row; in each aligned block of 256 rows (0 to 255, 256 to 511, ...) at most 68 rows name the same one
- route_weights: float32 [2048, 2], P('ep'), may hold values from 0.1 to 1
- gate_w: bfloat16 [8, 2048, 3584], P('ep', None, 'tp'), may hold values from -0.125 to 0.125
- up_w: bfloat16 [8, 2048, 3584], P('ep', None, 'tp'), may hold values from -0.125 to 0.125
- down_w: bfloat16 [8, 3584, 2048], P('ep', 'tp'), may hold values from -0.09375 to 0.09375
Outputs:
- mixed: bfloat16 [4096, 2048], P(('ep', 'tp'))
- moe_out: bfloat16 [2048, 2048], P('ep', 'tp')
Inputs may be any that keep to these rules, and one draw needn't show every extreme that they name: `routes`: among the rows of one index of ep, no expert is named by more than 68 entries, a bound that some block reaches; a row names 2 different experts.
All inputs are finite; a program needn't handle non-finite values.
Results may differ from a plain program's by a relative error of at most 0.025.
Values may be sent and summed in bfloat16 or wider, within the bound.
A program may use at most 128 MiB of HBM per device.

v0:
```python
import math
import jax
import jax.numpy as jnp
from jax import lax
from jax.sharding import PartitionSpec as P

D = 2048
NOPE = 64
SEQS = 1
eps = 1e-06
rope_base = 10000.0
neg_big = -1e30


def rotate(values, positions):
    half_dim = values.shape[-1] // 2
    inv_freq = rope_base ** (-jnp.arange(half_dim, dtype=jnp.float32) * 2.0 / values.shape[-1])
    angles = positions.astype(jnp.float32)[:, None] * inv_freq[None, :]
    angles = angles.reshape((angles.shape[0],) + (1,) * (values.ndim - 2) + (half_dim,))
    cosine = jnp.cos(angles)
    sine_part = jnp.sin(angles)
    first_half = values[..., :half_dim].astype(jnp.float32)
    second_half = values[..., half_dim:].astype(jnp.float32)
    return jnp.concatenate(
        [
            first_half * cosine - second_half * sine_part,
            second_half * cosine + first_half * sine_part,
        ],
        axis=-1,
    )


def shards(
    queries,
    kv_latent,
    rope_key,
    kv_gain,
    kv_up,
    mix_out,
    moe_in,
    moe_gain,
    routes,
    route_weights,
    gate_w,
    up_w,
    down_w,
):
    block_rows = queries.shape[0]
    heads_here = queries.shape[1]
    value_dim = kv_up.shape[-1] - NOPE
    seq_len = block_rows * lax.axis_size("ep") // SEQS
    query_start = lax.axis_index("ep") * block_rows
    query_index = query_start + jnp.arange(block_rows, dtype=jnp.int32)
    seq_start = query_start // seq_len * seq_len
    query_nope = queries[..., :NOPE]
    query_rot = rotate(queries[..., NOPE:], query_index % seq_len).astype(jnp.bfloat16)
    score_scale = 1.0 / math.sqrt(queries.shape[-1])
    initial = (
        jnp.full((block_rows, heads_here), neg_big, jnp.float32),
        jnp.zeros((block_rows, heads_here), jnp.float32),
        jnp.zeros((block_rows, heads_here, value_dim), jnp.float32),
    )
    latent_piece = lax.all_gather(kv_latent, ("ep", "tp"), axis=0, tiled=True)
    rope_piece = lax.all_gather(rope_key, ("ep", "tp"), axis=0, tiled=True)
    piece_rows = latent_piece.shape[0]
    sub_rows = math.gcd(piece_rows, 512)

    def sub_block(state_in, offset):

        def attend_piece(state_run):
            running_max, running_sum, weighted = state_run
            latent_rows = lax.dynamic_slice_in_dim(latent_piece, offset, sub_rows, 0).astype(
                jnp.float32
            )
            rope_rows = lax.dynamic_slice_in_dim(rope_piece, offset, sub_rows, 0)
            key_ids = offset + jnp.arange(sub_rows, dtype=jnp.int32)
            normed = (
                latent_rows
                * lax.rsqrt(jnp.mean(latent_rows * latent_rows, axis=-1, keepdims=True) + eps)
                * kv_gain
            ).astype(jnp.bfloat16)
            head_proj = jnp.einsum(
                "nr,rhd->nhd", normed, kv_up, preferred_element_type=jnp.float32
            ).astype(jnp.bfloat16)
            key_rot = rotate(rope_rows, key_ids % seq_len).astype(jnp.bfloat16)
            scores = jnp.einsum(
                "qhd,khd->qhk",
                query_nope,
                head_proj[..., :NOPE],
                preferred_element_type=jnp.float32,
            )
            scores = (
                scores
                + jnp.einsum("qhd,kd->qhk", query_rot, key_rot, preferred_element_type=jnp.float32)
            ) * score_scale
            allowed = (
                (key_ids[None, :] <= query_index[:, None]) & (key_ids[None, :] >= seq_start)
            )[:, None, :]
            scores = jnp.where(allowed, scores, neg_big)
            new_max = jnp.maximum(running_max, jnp.max(scores, axis=-1))
            exp_scores = jnp.where(allowed, jnp.exp(scores - new_max[..., None]), 0.0)
            rescale = jnp.exp(running_max - new_max)
            running_sum = running_sum * rescale + jnp.sum(exp_scores, axis=-1)
            weighted = weighted * rescale[..., None] + jnp.einsum(
                "qhk,khd->qhd",
                exp_scores.astype(jnp.bfloat16),
                head_proj[..., NOPE:],
                preferred_element_type=jnp.float32,
            )
            return (new_max, running_sum, weighted)

        is_needed = (offset < query_start + block_rows) & (offset + sub_rows > seq_start)
        return (lax.cond(is_needed, attend_piece, lambda state_run: state_run, state_in), None)

    state_out, _ = lax.scan(
        sub_block, initial, jnp.arange(0, piece_rows, sub_rows, dtype=jnp.int32)
    )
    running_max, running_sum, weighted = state_out
    attn = (weighted / running_sum[..., None]).astype(jnp.bfloat16)
    mixed = lax.psum_scatter(
        jnp.einsum("thv,hvd->td", attn, mix_out, preferred_element_type=jnp.float32).astype(
            jnp.bfloat16
        ),
        "tp",
        scatter_dimension=0,
        tiled=True,
    )
    rows_here = routes.shape[0]
    top_count = routes.shape[1]
    experts = gate_w.shape[0] * lax.axis_size("ep")
    mean_slots = top_count * rows_here // experts
    capacity = mean_slots + max(mean_slots // 16, 1)
    flat_routes = routes.reshape(-1)
    onehot = (flat_routes[:, None] == jnp.arange(experts, dtype=jnp.int32)[None, :]).astype(
        jnp.int32
    )
    slot_rank = jnp.sum((jnp.cumsum(onehot, axis=0) - onehot) * onehot, axis=1)
    slot_dest = flat_routes * capacity + slot_rank
    slot_owner = (
        jnp.full((experts * capacity,), -1, jnp.int32)
        .at[slot_dest]
        .set(jnp.arange(rows_here * top_count, dtype=jnp.int32))
    )
    is_valid = slot_owner >= 0
    token_row = jnp.maximum(slot_owner, 0) // top_count
    send_rows = jnp.where(is_valid[:, None], moe_in[token_row], 0).reshape(
        experts, capacity, moe_in.shape[1]
    )
    arrived = lax.all_to_all(send_rows, "ep", split_axis=0, concat_axis=0, tiled=True)
    piece_f = lax.all_gather(arrived, "tp", axis=2, tiled=True).astype(jnp.float32)
    scaled = (piece_f * moe_gain).astype(jnp.bfloat16)
    gate_rows = gate_w[0]
    up_rows = up_w[0]
    gate_acc = jnp.einsum("scd,df->scf", scaled, gate_rows, preferred_element_type=jnp.float32)
    up_acc = jnp.einsum("scd,df->scf", scaled, up_rows, preferred_element_type=jnp.float32)
    squares = jnp.sum(piece_f * piece_f, axis=-1)
    gate_acc, up_acc, squares = (gate_acc, up_acc, squares)
    row_scale = lax.rsqrt(squares / D + eps)[..., None]
    hidden = (jax.nn.silu(gate_acc * row_scale) * (up_acc * row_scale)).astype(jnp.bfloat16)
    partial_value = jnp.einsum("scf,fd->scd", hidden, down_w[0], preferred_element_type=jnp.float32)
    summed = lax.psum_scatter(
        partial_value.astype(jnp.bfloat16), "tp", scatter_dimension=2, tiled=True
    )
    returned = lax.all_to_all(summed, "ep", split_axis=0, concat_axis=0, tiled=True)
    flat_back = returned.reshape(experts * capacity, returned.shape[-1])
    picked = (
        flat_back[slot_dest].astype(jnp.float32).reshape(rows_here, top_count, returned.shape[-1])
    )
    moe_out = jnp.sum(picked * route_weights[..., None], axis=1).astype(jnp.bfloat16)
    return (mixed, moe_out)


def solution(mesh):
    in_specs = (
        P("ep", "tp", None),
        P(("ep", "tp"), None),
        P(("ep", "tp"), None),
        P(),
        P(None, "tp", None),
        P("tp", None, None),
        P("ep", "tp"),
        P(),
        P("ep", None),
        P("ep", None),
        P("ep", None, "tp"),
        P("ep", None, "tp"),
        P("ep", "tp", None),
    )
    out_specs = (P(("ep", "tp"), None), P("ep", "tp"))
    return jax.shard_map(shards, mesh=mesh, in_specs=in_specs, out_specs=out_specs, check_vma=False)
```

profile of v0, /device:TPU:0, one launch (start us, length us, event | category | flops | bytes accessed | tf_op | source)
XLA Modules:
  0.0 246.8 jit_solution(13989375117769268064)
XLA Ops:
  7.2 0.9 copy.21
  9.1 1.1 reduce-window.6
  10.9 2.4 scatter_custom_fusion
  13.4 2.7 %gather_fusion = bf16[544,512]{1,0:T(8,128)(2,1)S(1)} fusion(bf16[256,512]{1,0:T(8,128)(2,1)S(1)} %copy-done.1, s32[1024]{0:T(1024)S(1)} %pad_clamp_fusion.1), kind=kCustom, calls=%fused_computation | custom fusion | bytes 1116288 | tf_op jit(solution)/shard_map/gather | solution.py:146
  16.5 23.7 %all_to_all.10 = bf16[8,68,512]{2,1,0:T(8,128)(2,1)} all-to-all(bf16[8,68,512]{2,1,0:T(8,128)(2,1)S(1)} %broadcast_select_fusion), channel_id=1, replica_groups=mesh['ep'=8,'tp'=4] {'ep'}, dimensions={0} | all-to-all | bytes 1114112 | tf_op jit(solution)/shard_map/all_to_all | solution.py:149
  41.0 21.8 %all-gather.5.cloned.1.call-done = bf16[8,68,2048]{2,1,0:T(8,128)(2,1)} async-done(((bf16[8,68,512]{2,1,0:T(8,128)(2,1)}), bf16[8,68,2048]{2,1,0:T(8,128)(2,1)}) %all-gather.5.cloned.1.call-update) | async-done | bytes 2228240 | tf_op jit(solution)/shard_map/all_gather | solution.py:150
  62.9 2.4 fusion.39
  65.3 6.0 %fusion.42 = f32[8,68,896]{2,1,0:T(8,128)} fusion(bf16[1,2048,896]{2,1,0:T(8,128)(2,1)} %param.28, bf16[8,68,2048]{2,1,0:T(8,128)(2,1)S(1)} %copy-done.2, f32[2048]{0:T(1024)S(1)} %copy-done.8), kind=kOutput, calls=%fused_computation.63 | convolution fusion | flops 1999831040 | bytes 7856128 | tf_op jit(solution)/shard_map/scd,df->scf/dot_general | solution.py:155
  71.3 10.5 %fusion.46 = bf16[8,68,2048]{2,1,0:T(8,128)(2,1)} fusion(bf16[1,896,2048]{2,1,0:T(8,128)(2,1)} %param.29, f32[8,68,896]{2,1,0:T(8,128)} %fusion.42, bf16[1,2048,896]{2,1,0:T(8,128)(2,1)} %param.27, bf16[8,68,2048]{2,1,0:T(8,128)(2,1)S(1)} %copy-done.2, f32[2048]{0:T(1024)S(1)} %copy-done.8, f32[8,68]{1,0:T(8,128)S(1)} %add_rsqrt_fusion.1), kind=kOutput, calls=%fused_computation.67 | convolution fusion | flops 4001333248 | bytes 13756544 | tf_op jit(solution)/shard_map/scf,fd->scd/dot_general | solution.py:160
  81.9 0.8 copy-done.3
  83.2 44.1 %all_gather.10 = bf16[4096,32]{0,1:T(8,128)(2,1)} all-gather(bf16[128,32]{0,1:T(8,128)(2,1)S(1)} %copy-done.6), channel_id=1, replica_groups=mesh['ep'=8,'tp'=4] {'ep','tp'}, dimensions={0}, use_global_device_ids=true | all-gather | bytes 270336 | tf_op jit(solution)/shard_map/all_gather | solution.py:64
  127.3 22.8 %while.17 = (s32[]{:T(128)}, f32[512,2]{0,1:T(2,128)S(1)}, f32[512,2]{0,1:T(2,128)S(1)}, f32[512,2,64]{0,2,1:T(8,128)S(1)}, s32[8]{0:T(128)S(1)}, /*index=5*/s32...) while((s32[]{:T(128)}, f32[512,2]{0,1:T(2,128)S(1)}, ...), condition=%wide.region_6.7_spmd.clone, body=%wide.region_0.6_spmd.clone.sunk | while | flops 207981088 | bytes 14346293 | solution.py:115
  129.0 8.8 %conditional.3 = ((f32[512,2]{0,1:T(2,128)S(1)}, f32[512,2]{0,1:T(2,128)S(1)}, f32[512,2,64]{0,2,1:T(8,128)S(1)})) conditional(s32[]{:T(128)} %convert_element_type.174, (f32[512,2]{0,1:T(2,128)S(1)}, f32[512,2]{0,1:T(2,128)S(1)}, f32[512,2,64]{0,2,1:T(8,128)S(1)}) %tuple.51, (s32[]{:T(128)}, s32[]{:T(128)}, s32[]{:T(128)}, ...), branch_computations={%region_1.1_spmd, %region_2.5_spmd} | conditional | flops 207981088 | bytes 14343918 | solution.py:113
  130.7 1.1 fusion.11
  131.8 1.2 fusion.14
  134.2 1.0 fusion.27
  136.0 0.7 fusion.75
  150.2 2.1 bitcast_convert_fusion
  152.2 1.7 reduce-scatter.5.cloned.1.call-done
  153.9 59.0 %all-to-all-start.1 = ((bf16[8,68,512]{2,1,0:T(8,128)(2,1)}), bf16[8,68,512]{2,1,0:T(8,128)(2,1)S(1)}, u32[]{:S(2)}, u32[]{:S(2)}) async-start(bf16[8,68,512]{2,1,0:T(8,128)(2,1)} %reduce-scatter.5.cloned.1.call-done), calls=%async_computation.3 | async-start | bytes 1179648 | tf_op jit(solution)/shard_map/all_to_all | solution.py:164
  213.1 16.2 %all-to-all-done.1 = bf16[8,68,512]{2,1,0:T(8,128)(2,1)S(1)} async-done(((bf16[8,68,512]{2,1,0:T(8,128)(2,1)}), bf16[8,68,512]{2,1,0:T(8,128)(2,1)S(1)}, u32[]{:S(2)}, u32[]{:S(2)}) %all-to-all-start.1) | async-done | bytes 557088 | tf_op jit(solution)/shard_map/all_to_all | solution.py:164
  229.4 2.0 gather_fusion.1
  232.1 2.1 multiply_reduce_fusion
  234.1 6.1 %reduce-scatter.3.cloned.1.call-done = bf16[128,2048]{1,0:T(8,128)(2,1)} async-done(((bf16[512,2048]{1,0:T(8,128)(2,1)}), bf16[128,2048]{1,0:T(8,128)(2,1)}) %reduce-scatter.3.cloned.1.call-update) | async-done | bytes 524304 | tf_op jit(solution)/shard_map/reduce_scatter | solution.py:120
  (96 shorter events, 12.0 us)
Async XLA Ops:
  7.2 143.0 %copy-start = (bf16[2,64,2048]{2,1,0:T(8,128)(2,1)S(1)}, bf16[2,64,2048]{2,1,0:T(8,128)(2,1)}, u32[]{:S(2)}) copy-start(bf16[2,64,2048]{2,1,0:T(8,128)(2,1)} %param.22) | copy-start | bytes 1572868
  7.2 6.2 %copy-start.1 = (bf16[256,512]{1,0:T(8,128)(2,1)S(1)}, bf16[256,512]{1,0:T(8,128)(2,1)}, u32[]{:S(2)}) copy-start(bf16[256,512]{1,0:T(8,128)(2,1)} %param.23) | copy-start | bytes 786436
  7.2 55.7 %all-gather.5.cloned.1.call-start = ((), (), s32[]{:S(2)}) async-start(), calls=%async_computation.6 | async-start | bytes 2949120 | tf_op jit(solution)/shard_map/all_gather | solution.py:150
  16.5 48.8 %copy-start.8 = (f32[2048]{0:T(1024)S(1)}, f32[2048]{0:T(1024)}, u32[]{:S(2)}) copy-start(f32[2048]{0:T(1024)} %param.24) | copy-start | bytes 24580
  40.2 87.0 %all-gather.3.cloned.1.call-start = ((), (), s32[]{:S(2)}) async-start(), calls=%async_computation.4 | async-start | bytes 1081344 | tf_op jit(solution)/shard_map/all_gather | solution.py:63
  41.0 112.9 %reduce-scatter.5.cloned.1.call-start = ((), (), s32[]{:S(2)}) async-start(), calls=%async_computation.7 | async-start | bytes 2949120 | tf_op jit(solution)/shard_map/reduce_scatter | solution.py:161
  62.9 2.4 copy-start.2
  81.8 0.9 copy-start.3
  81.8 0.9 copy-start.4
  81.8 1.4 copy-start.6
  81.8 45.5 %copy-start.5 = (f32[128]{0:T(128)S(1)}, f32[128]{0:T(128)}, u32[]{:S(2)}) copy-start(f32[128]{0:T(128)} %param.20) | copy-start | bytes 1540
  81.8 158.5 %reduce-scatter.3.cloned.1.call-start = ((), (), s32[]{:S(2)}) async-start(), calls=%async_computation.5 | async-start | bytes 2621440 | tf_op jit(solution)/shard_map/reduce_scatter | solution.py:120
  152.2 60.7 %copy-start.7 = (f32[256,2]{0,1:T(2,128)S(1)}, f32[256,2]{0,1:T(2,128)}, u32[]{:S(2)}) copy-start(f32[256,2]{0,1:T(2,128)} %param.26) | copy-start | bytes 6148
  153.9 75.4 %all-to-all-start.1 = ((bf16[8,68,512]{2,1,0:T(8,128)(2,1)}), bf16[8,68,512]{2,1,0:T(8,128)(2,1)S(1)}, u32[]{:S(2)}, u32[]{:S(2)}) async-start(bf16[8,68,512]{2,1,0:T(8,128)(2,1)} %reduce-scatter.5.cloned.1.call-done), calls=%async_computation.3 | async-start | bytes 1179648 | tf_op jit(solution)/shard_map/all_to_all | solution.py:164
Sparse Core Ops, SparseCore 0:
  40.4 22.4 all-gather.4
  65.8 53.8 all-gather.2
  122.2 31.7 reduce-scatter.4
  156.9 83.3 reduce-scatter.2
where the time goes:
time: 248 us; the launch traced here: 247 us
  blocking collectives  67.8 us (27%)
  starting transfers between devices  59.1 us (24%)
  waiting for transfers between devices  46.7 us (19%)
  matrix products  21.6 us (9%)
  local copies, waits for them, and re-layouts  15.6 us (6%)
  between operations  14.1 us (6%)
  loops' own time  11.2 us (5%)
  other arithmetic  10.8 us (4%)
    all_to_all x1, starting transfers between devices, shards(): lax.all_to_all(summed, 'ep', split_axis=0, concat_axis=0, tiled=True)  59 us
    all_gather x1, blocking collectives, shards(): rope_piece = lax.all_gather(rope_key, ('ep', 'tp'), axis=0, tiled=True)  44.1 us
    all_to_all x1, blocking collectives, shards(): lax.all_to_all(send_rows, 'ep', split_axis=0, concat_axis=0, tiled=True)  23.7 us
    all_gather x1, waiting for transfers between devices, shards(): lax.all_gather(arrived, 'tp', axis=2, tiled=True).astype(jnp.float32)  21.8 us
    all_to_all x1, waiting for transfers between devices, shards(): lax.all_to_all(summed, 'ep', split_axis=0, concat_axis=0, tiled=True)  16.2 us
    dot_general x1, matrix products, shards(): jnp.einsum('scf,fd->scd', hidden, down_w[0], preferred_element_type=jnp.f...  10.5 us
    another operation x1, loops' own time, shards(): lax.scan(sub_block, initial, jnp.arange(0, piece_rows, sub_rows, dtype=jn...  9.28 us
    reduce_scatter x1, waiting for transfers between devices, shards(): lax.psum_scatter(jnp.einsum('thv,hvd->td', attn, mix_out, preferred_eleme...  6.14 us
  transfers between devices with their start and end apart: 5, of which 4 were waited for; matrix products, arithmetic and copies ran while one was open for 15% of the time, Pallas kernels for 0%

commit v1 on v0

--- a/solution.py
+++ b/solution.py
@@ -10,6 +10,11 @@
 eps = 1e-06
 rope_base = 10000.0
 neg_big = -1e30
+
+
+def stack_and_merge(x, axis, dim):
+    tiles = lax.all_gather(x, axis)
+    return jnp.concatenate(tiles, axis=dim)
 
 
 def rotate(values, positions):
@@ -147,7 +152,7 @@
         experts, capacity, moe_in.shape[1]
     )
     arrived = lax.all_to_all(send_rows, "ep", split_axis=0, concat_axis=0, tiled=True)
-    piece_f = lax.all_gather(arrived, "tp", axis=2, tiled=True).astype(jnp.float32)
+    piece_f = stack_and_merge(arrived, "tp", 2).astype(jnp.float32)
     scaled = (piece_f * moe_gain).astype(jnp.bfloat16)
     gate_rows = gate_w[0]
     up_rows = up_w[0]

time: 248 us -> 257 us (1.036)
  local copies, waits for them, and re-layouts: 15.6 us -> 20.1 us
  other arithmetic: 10.8 us -> 15.1 us
  blocking collectives: 67.8 us -> 65.1 us
    convert_element_type x0 -> x2, other arithmetic: none -> 4.85 us  [the longest x1 4.24 us: shards(): scaled = (piece_f * moe_gain).astype(jnp.bfloat16)]
    convert_element_type x0 -> x1, local copies, waits for them, and re-layouts: none -> 3 us  [shards(): scaled = (piece_f * moe_gain).astype(jnp.bfloat16)]
    all_gather x1, blocking collectives: 44.1 us -> 41.4 us  [shards(): rope_piece = lax.all_gather(rope_key, ('ep', 'tp'), axis=0, tiled=True)]
  transfers between devices with their start and end apart: 5 -> 5, of which waited for: 4 -> 3; matrix products, arithmetic and copies ran while one was open for 15% -> 19% of each run, Pallas kernels for 0% -> 0%
where the time goes in v1:
time: 257 us; the launch traced here: 255 us
  blocking collectives  65.1 us (25%)
  starting transfers between devices  59.9 us (23%)
  waiting for transfers between devices  44.2 us (17%)
  matrix products  23.4 us (9%)
  local copies, waits for them, and re-layouts  20.1 us (8%)
  other arithmetic  15.1 us (6%)
  between operations  14.1 us (5%)
  loops' own time  13.7 us (5%)
    all_to_all x1, starting transfers between devices, shards(): lax.all_to_all(summed, 'ep', split_axis=0, concat_axis=0, tiled=True)  59.7 us
    all_gather x1, blocking collectives, shards(): rope_piece = lax.all_gather(rope_key, ('ep', 'tp'), axis=0, tiled=True)  41.4 us
    all_to_all x1, blocking collectives, shards(): lax.all_to_all(send_rows, 'ep', split_axis=0, concat_axis=0, tiled=True)  23.6 us
    all_gather x1, waiting for transfers between devices, stack_and_merge(): tiles = lax.all_gather(x, axis)  21.1 us
    all_to_all x1, waiting for transfers between devices, shards(): lax.all_to_all(summed, 'ep', split_axis=0, concat_axis=0, tiled=True)  16.2 us
    another operation x1, loops' own time, shards(): lax.scan(sub_block, initial, jnp.arange(0, piece_rows, sub_rows, dtype=jn...  11.4 us
    dot_general x1, matrix products, shards(): jnp.einsum('scf,fd->scd', hidden, down_w[0], preferred_element_type=jnp.f...  11 us
    dot_general x1, matrix products, shards(): jnp.einsum('scd,df->scf', scaled, up_rows, preferred_element_type=jnp.flo...  7.25 us
  transfers between devices with their start and end apart: 5, of which 3 were waited for; matrix products, arithmetic and copies ran while one was open for 19% of the time, Pallas kernels for 0%

profile of v1, /device:TPU:0, one launch (start us, length us, event | category | flops | bytes accessed | tf_op | source)
XLA Modules:
  0.0 255.5 jit_solution(5770789361233274126)
XLA Ops:
  7.2 0.8 broadcast_multiply_fusion
  8.0 0.8 copy.51
  9.4 1.1 reduce-window.6
  10.9 2.4 scatter_custom_fusion
  13.5 2.7 %gather_fusion = bf16[544,512]{1,0:T(8,128)(2,1)S(1)} fusion(bf16[256,512]{1,0:T(8,128)(2,1)S(1)} %copy-done.1, s32[1024]{0:T(1024)S(1)} %pad_clamp_fusion.1), kind=kCustom, calls=%fused_computation | custom fusion | bytes 1116288 | tf_op jit(solution)/shard_map/gather | solution.py:151
  16.5 23.6 %all_to_all.10 = bf16[8,68,512]{2,1,0:T(8,128)(2,1)S(1)} all-to-all(bf16[8,68,512]{2,1,0:T(8,128)(2,1)S(1)} %broadcast_select_fusion), channel_id=1, replica_groups=mesh['ep'=8,'tp'=4] {'ep'}, dimensions={0} | all-to-all | bytes 1114112 | tf_op jit(solution)/shard_map/all_to_all | solution.py:154
  40.1 1.0 copy.53
  42.0 21.1 %all-gather.6.cloned.1.call-done = bf16[32,68,512]{2,0,1:T(8,128)(2,1)} async-done(((bf16[8,68,512]{2,0,1:T(8,128)(2,1)}), bf16[32,68,512]{2,0,1:T(8,128)(2,1)}) %all-gather.6.cloned.1.call-update) | async-done | bytes 2228240 | tf_op jit(solution)/shard_map/all_gather | solution.py:16
  63.0 2.3 multiply_reduce_fusion
  66.0 4.2 %fusion.48 = bf16[8,68,4,512]{3,2,0,1:T(4,128)(2,1)S(1)} fusion(f32[4,8,68,512]{3,1,0,2:T(8,128)S(1)} %bitcast_convert_fusion.1, f32[4,512]{1,0:T(4,128)S(1)} %mul.201), kind=kLoop, calls=%fused_computation.67 | loop fusion | flops 2228224 | bytes 6692864 | tf_op jit(solution)/shard_map/convert_element_type | solution.py:156
  70.3 3.0 %convert_element_type.103 = bf16[8,68,2048]{2,0,1:T(8,128)(2,1)} reshape(bf16[8,68,4,512]{3,2,0,1:T(4,128)(2,1)S(1)} %fusion.48) | data formatting | bytes 4456448 | tf_op jit(solution)/shard_map/convert_element_type | solution.py:156
  73.3 7.3 %fusion.41 = f32[8,68,896]{2,1,0:T(8,128)} fusion(bf16[1,2048,896]{2,1,0:T(8,128)(2,1)} %param.28, bf16[8,68,2048]{2,0,1:T(8,128)(2,1)} %convert_element_type.103), kind=kOutput, calls=%fused_computation.62 | convolution fusion | flops 1996488704 | bytes 7847936 | tf_op jit(solution)/shard_map/scd,df->scf/dot_general | solution.py:160
  80.5 11.0 %fusion.45 = bf16[8,68,2048]{2,1,0:T(8,128)(2,1)} fusion(bf16[1,896,2048]{2,1,0:T(8,128)(2,1)} %param.29, f32[8,68,896]{2,1,0:T(8,128)} %fusion.41, bf16[1,2048,896]{2,1,0:T(8,128)(2,1)} %param.27, bf16[8,68,2048]{2,0,1:T(8,128)(2,1)S(1)} %copy-done.3, f32[8,68]{1,0:T(8,128)S(1)} %add_rsqrt_fusion.1), kind=kOutput, calls=%fused_computation.66 | convolution fusion | flops 3997990912 | bytes 13748352 | tf_op jit(solution)/shard_map/scf,fd->scd/dot_general | solution.py:165
  92.8 41.4 %all_gather.13 = bf16[4096,32]{0,1:T(8,128)(2,1)S(1)} all-gather(bf16[128,32]{0,1:T(8,128)(2,1)S(1)} %copy-done.7), channel_id=1, replica_groups=mesh['ep'=8,'tp'=4] {'ep','tp'}, dimensions={0}, use_global_device_ids=true | all-gather | bytes 270336 | tf_op jit(solution)/shard_map/all_gather | solution.py:69
  134.3 25.5 %while.17 = (s32[]{:T(128)}, f32[512,2]{0,1:T(2,128)S(1)}, f32[512,2]{0,1:T(2,128)S(1)}, f32[512,2,64]{0,2,1:T(8,128)S(1)}, s32[8]{0:T(128)S(1)}, /*index=5*/s32...) while((s32[]{:T(128)}, f32[512,2]{0,1:T(2,128)S(1)}, ...), condition=%wide.region_6.7_spmd.clone, body=%wide.region_0.6_spmd.clone.sunk | while | flops 207981088 | bytes 14346301 | solution.py:120
  136.4 8.7 %conditional.3 = ((f32[512,2]{0,1:T(2,128)S(1)}, f32[512,2]{0,1:T(2,128)S(1)}, f32[512,2,64]{0,2,1:T(8,128)S(1)})) conditional(s32[]{:T(128)} %convert_element_type.172, (f32[512,2]{0,1:T(2,128)S(1)}, f32[512,2]{0,1:T(2,128)S(1)}, f32[512,2,64]{0,2,1:T(8,128)S(1)}) %tuple.54, (s32[]{:T(128)}, s32[]{:T(128)}, s32[]{:T(128)}, ...), branch_computations={%region_1.1_spmd, %region_2.5_spmd} | conditional | flops 207981088 | bytes 14343918 | solution.py:118
  139.2 1.1 fusion.11
  140.2 1.2 fusion.14
  159.8 2.1 bitcast_convert_fusion
  161.9 59.7 %all-to-all-start.1 = ((bf16[8,68,512]{2,1,0:T(8,128)(2,1)}), bf16[8,68,512]{2,1,0:T(8,128)(2,1)S(1)}, u32[]{:S(2)}, u32[]{:S(2)}) async-start(bf16[8,68,512]{2,1,0:T(8,128)(2,1)} %reduce-scatter.5.cloned.1.call-done), calls=%async_computation.3 | async-start | bytes 1179648 | tf_op jit(solution)/shard_map/all_to_all | solution.py:169
  221.8 16.2 %all-to-all-done.1 = bf16[8,68,512]{2,1,0:T(8,128)(2,1)S(1)} async-done(((bf16[8,68,512]{2,1,0:T(8,128)(2,1)}), bf16[8,68,512]{2,1,0:T(8,128)(2,1)S(1)}, u32[]{:S(2)}, u32[]{:S(2)}) %all-to-all-start.1) | async-done | bytes 557088 | tf_op jit(solution)/shard_map/all_to_all | solution.py:169
  238.1 2.0 gather_fusion.1
  240.8 2.1 multiply_reduce_fusion.1
  242.8 6.1 %reduce-scatter.3.cloned.1.call-done = bf16[128,2048]{1,0:T(8,128)(2,1)} async-done(((bf16[512,2048]{1,0:T(8,128)(2,1)}), bf16[128,2048]{1,0:T(8,128)(2,1)}) %reduce-scatter.3.cloned.1.call-update) | async-done | bytes 524304 | tf_op jit(solution)/shard_map/reduce_scatter | solution.py:125
  (104 shorter events, 14.6 us)
Async XLA Ops:
  7.2 152.6 %copy-start = (bf16[2,64,2048]{2,1,0:T(8,128)(2,1)S(1)}, bf16[2,64,2048]{2,1,0:T(8,128)(2,1)}, u32[]{:S(2)}) copy-start(bf16[2,64,2048]{2,1,0:T(8,128)(2,1)} %param.22) | copy-start | bytes 1572868
  7.2 6.3 %copy-start.1 = (bf16[256,512]{1,0:T(8,128)(2,1)S(1)}, bf16[256,512]{1,0:T(8,128)(2,1)}, u32[]{:S(2)}) copy-start(bf16[256,512]{1,0:T(8,128)(2,1)} %param.23) | copy-start | bytes 786436
  7.2 55.9 %all-gather.6.cloned.1.call-start = ((), (), s32[]{:S(2)}) async-start(), calls=%async_computation.7 | async-start | bytes 2785280 | tf_op jit(solution)/shard_map/all_gather | solution.py:16
  16.4 25.6 %copy-start.8 = (f32[2048]{0:T(1024)S(1)}, f32[2048]{0:T(1024)}, u32[]{:S(2)}) copy-start(f32[2048]{0:T(1024)} %param.24) | copy-start | bytes 24580
  41.1 93.1 %all-gather.4.cloned.1.call-start = ((), (), s32[]{:S(2)}) async-start(), calls=%async_computation.4 | async-start | bytes 1081344 | tf_op jit(solution)/shard_map/all_gather | solution.py:68
  41.9 120.0 %reduce-scatter.5.cloned.1.call-start = ((), (), s32[]{:S(2)}) async-start(), calls=%async_computation.6 | async-start | bytes 2949120 | tf_op jit(solution)/shard_map/reduce_scatter | solution.py:166
  63.0 2.4 copy-start.2
  73.3 7.3 %copy-start.3 = (bf16[8,68,2048]{2,0,1:T(8,128)(2,1)S(1)}, bf16[8,68,2048]{2,0,1:T(8,128)(2,1)}, u32[]{:S(2)}) copy-start(bf16[8,68,2048]{2,0,1:T(8,128)(2,1)} %convert_element_type.103) | copy-start | bytes 6684676
  91.5 0.8 copy-start.5
  91.5 1.0 copy-start.4
  91.5 1.3 copy-start.7
  91.5 42.8 %copy-start.6 = (f32[128]{0:T(128)S(1)}, f32[128]{0:T(128)}, u32[]{:S(2)}) copy-start(f32[128]{0:T(128)} %param.20) | copy-start | bytes 1540
  91.5 157.4 %reduce-scatter.3.cloned.1.call-start = ((), (), s32[]{:S(2)}) async-start(), calls=%async_computation.5 | async-start | bytes 2621440 | tf_op jit(solution)/shard_map/reduce_scatter | solution.py:125
  161.9 59.8 %copy-start.9 = (f32[256,2]{0,1:T(2,128)S(1)}, f32[256,2]{0,1:T(2,128)}, u32[]{:S(2)}) copy-start(f32[256,2]{0,1:T(2,128)} %param.26) | copy-start | bytes 6148
  161.9 76.1 %all-to-all-start.1 = ((bf16[8,68,512]{2,1,0:T(8,128)(2,1)}), bf16[8,68,512]{2,1,0:T(8,128)(2,1)S(1)}, u32[]{:S(2)}, u32[]{:S(2)}) async-start(bf16[8,68,512]{2,1,0:T(8,128)(2,1)} %reduce-scatter.5.cloned.1.call-done), calls=%async_computation.3 | async-start | bytes 1179648 | tf_op jit(solution)/shard_map/all_to_all | solution.py:169
Sparse Core Ops, SparseCore 0:
  41.3 21.7 all-gather.5
  65.9 53.9 all-gather.3
  122.4 31.6 reduce-scatter.4
  162.0 86.8 reduce-scatter.2
